TPU v7x, 32 devices: a whole 2x2x4 slice. The times are simulated.
32 devices in a mesh: ep: 8 (over z, x), tp: 4 (over y, core).
Axes of the slice: x: 2, y: 2, z: 4, core: 2. Of those that a mesh axis runs over, the one named last changes fastest.
Arguments:
- tokens: bfloat16 [4608, 2048], P(('ep', 'tp')), may hold values from -6 to 6
- norm_gain: float32 [2048], replicated, may hold values from 0.1 to 1.9
- expert_ids: int32 [4608, 8], P(('ep', 'tp')), may hold values from 0 to 15, all different within a row; in each aligned block of 144 rows (0 to 143, 144 to 287, ...) at most 144 rows name the same one
- route_weights: float32 [4608, 8], P(('ep', 'tp')), may hold values from 0.3 to 1
- expert_gate: bfloat16 [16, 512, 2048], P('ep', 'tp'), may hold values from -0.125 to 0.125
- expert_up: bfloat16 [16, 512, 2048], P('ep', 'tp'), may hold values from -0.125 to 0.125
- expert_down: bfloat16 [16, 512, 2048], P('ep', 'tp'), may hold values from -0.25 to 0.25
- shared_gate: bfloat16 [512, 2048], P('tp'), may hold values from -0.125 to 0.125
- shared_up: bfloat16 [512, 2048], P('tp'), may hold values from -0.125 to 0.125
- shared_down: bfloat16 [512, 2048], P('tp'), may hold values from -0.25 to 0.25
- side_in: bfloat16 [2048, 1024], P('ep'), may hold values from -0.125 to 0.125
- side_out: bfloat16 [2048, 1024], P('ep'), may hold values from -0.1875 to 0.1875
- side_gate: bfloat16 [2048], replicated, may hold values from -0.125 to 0.125
Outputs:
- mixed: bfloat16 [4608, 2048], P(('ep', 'tp'))
Inputs may be any that keep to these rules, and one draw needn't show every extreme that they name: `expert_ids`: each row names 8 different experts of 0 to 15; within the rows of one device (aligned blocks of 144 rows) no expert is named more than 144 times, and in some of those blocks some expert is named exactly 144 times.
All inputs are finite; a program needn't handle non-finite values.
Results may differ from a plain program's by a relative error of at most 0.0068.
Values may be sent and summed in bfloat16 or wider, within the bound.
A program may use at most 320 MiB of HBM per device.

v0:
```python
import functools

import jax
import jax.numpy as jnp
import numpy as np
from jax import lax
from jax.experimental import pallas as pl
from jax.experimental.pallas import tpu as pltpu
from jax.sharding import PartitionSpec as P

norm_eps = 1.0
MESH = pl.DeviceIdType.MESH
NT = (((1,), (1,)), ((), ()))


def silu(v):
    return v / (1.0 + jnp.exp(-v))


def kernel(
    dims,
    tokens_ref, gain_ref, ids_ref, route_ref, side_gate_ref, mask_ref,
    gate_ref, up_ref, down_ref, s_gate_ref, s_up_ref, s_down_ref, side_in_ref, side_out_ref,
    out_ref,
    tok, wg, wu, wd, side, hidden, side_hid, acc, xs, xr, sent, got,
    tok_send, tok_recv, w_send, w_recv, side_send, side_recv, swap_send, swap_recv, local_sem,
    x_send, x_recv, r_send, r_recv, l_send, l_recv,
):
    nz, nx, ny, nc, experts_all, local_experts, chunks = dims
    n_ep, n_tp = nz * nx, ny * nc
    me, tp = lax.axis_index("ep"), lax.axis_index("tp")
    z, x = me // nx, me % nx
    y, c = tp // nc, tp % nc
    rows = tokens_ref.shape[0]
    width = out_ref.shape[1]
    routed = gate_ref.shape[0]
    part, side_cols = wg.shape[1], side.shape[2]
    extra = part - routed
    piece = width // chunks
    side_rows = side.shape[1]

    def cols(q):
        return pl.ds(pl.multiple_of(q * piece, piece), piece)

    barrier = pltpu.get_barrier_semaphore()
    for j in range(1, n_ep):
        pl.semaphore_signal(barrier, inc=1, device_id=((me + j) % n_ep, tp), device_id_type=MESH)
    for j in range(1, n_tp):
        pl.semaphore_signal(barrier, inc=1, device_id=(me, (tp + j) % n_tp), device_id_type=MESH)
    pl.semaphore_wait(barrier, n_ep + n_tp - 2)

    def tok_rows(bz, bx):
        return pl.ds(pl.multiple_of((bx * nz + bz) * rows, rows), rows)

    def tok_copy(bz, way):
        if way < 2:
            target = (me + nx if way == 0 else me - nx, tp)
        else:
            target = (z * nx + (x + way - 1) % nx, tp)
        return pltpu.make_async_remote_copy(
            src_ref=tok.at[tok_rows(bz, x)],
            dst_ref=tok.at[tok_rows(bz, x)],
            send_sem=tok_send.at[bz, way],
            recv_sem=tok_recv.at[x * nz + bz],
            device_id=target,
            device_id_type=MESH,
        )

    def tok_wait(bz, bx):
        pltpu.make_async_remote_copy(
            src_ref=tok.at[tok_rows(bz, bx)],
            dst_ref=tok.at[tok_rows(bz, bx)],
            send_sem=tok_send.at[0, 0],
            recv_sem=tok_recv.at[bx * nz + bz],
            device_id=(me, tp),
            device_id_type=MESH,
        ).wait_recv()

    def w_place(k, owner):
        if k == 0:
            return wg.at[owner]
        if k == 1:
            return wu.at[owner]
        return wd.at[owner, :, cols(k - 2)]

    def own_parts(ref, shared_ref, place, q=None):
        at = pl.ds(pl.multiple_of(me * extra, extra), extra)
        at = at if shared_ref.shape[0] > extra else pl.ds(0, extra)
        head, tail = pl.ds(0, routed), pl.ds(routed, extra)
        if q is None:
            return (ref, place.at[head]), (shared_ref.at[at], place.at[tail])
        return (ref.at[:, q], place.at[head, q]), (shared_ref.at[at, q], place.at[tail, q])

    def w_parts(k):
        if k == 0:
            return own_parts(gate_ref, s_gate_ref, wg.at[tp])
        if k == 1:
            return own_parts(up_ref, s_up_ref, wu.at[tp])
        return own_parts(down_ref, s_down_ref, wd.at[tp], cols(k - 2))

    def w_copy(k, by, way, refs=None):
        if way < 2:
            target = (me, tp + nc if way == 0 else tp - nc)
        else:
            target = (me, y * nc + (c + way - 1) % nc)
        owner = by * nc + c
        src, dst = (w_place(k, owner), w_place(k, owner)) if refs is None else refs
        return pltpu.make_async_remote_copy(
            src_ref=src,
            dst_ref=dst,
            send_sem=w_send.at[k, by, way],
            recv_sem=w_recv.at[k, owner],
            device_id=target,
            device_id_type=MESH,
        )

    def w_wait(k, owner):
        pltpu.make_async_remote_copy(
            src_ref=w_place(k, owner), dst_ref=w_place(k, owner), send_sem=w_send.at[0, 0, 0],
            recv_sem=w_recv.at[k, owner], device_id=(me, tp), device_id_type=MESH,
        ).wait_recv()

    def side_source(ref, to):
        if len(ref.shape) == 3:
            return ref.at[to]
        return ref.at[:, pl.ds(pl.multiple_of(to * side_cols, side_cols), side_cols)]

    def side_copy(j, p):
        to = (me + j) % n_ep
        return pltpu.make_async_remote_copy(
            src_ref=side_source((side_in_ref, side_out_ref)[p], to),
            dst_ref=side.at[p * n_ep + me],
            send_sem=side_send.at[j],
            recv_sem=side_recv.at[me],
            device_id=(to, tp),
            device_id_type=MESH,
        )

    def side_each(act):
        for p in range(nc):

            @pl.when(c == p)
            def _():
                for j in range(1, n_ep):
                    act(side_copy(j, p))

    def side_own(p):
        return pltpu.make_async_copy(
            side_source((side_in_ref, side_out_ref)[p], me), side.at[p * n_ep + me],
            local_sem.at[3],
        )

    def swap_copy():
        half = side.at[pl.ds(c * n_ep, n_ep)]
        return pltpu.make_async_remote_copy(
            src_ref=half, dst_ref=half, send_sem=swap_send, recv_sem=swap_recv,
            device_id=(me, y * nc + 1 - c), device_id_type=MESH,
        )

    def each_own(copy_of, at, last, ways, act):
        @pl.when(at < last)
        def _():
            act(copy_of(0))

        @pl.when(at > 0)
        def _():
            act(copy_of(1))

        for way in range(2, ways):
            act(copy_of(way))

    def each_forward(copy_of, index_of, at, last, ways, step, act, arrive):
        @pl.when(at >= step)
        def _():
            b = at - step
            arrive(b)

            @pl.when(at < last)
            def _():
                act(copy_of(b, 0))

            for way in range(2, ways):
                act(copy_of(b, way))

        @pl.when(at + step <= last)
        def _():
            b = at + step
            arrive(b)

            @pl.when(at > 0)
            def _():
                act(copy_of(b, 1))

            for way in range(2, ways):
                act(copy_of(b, way))

    start = lambda copy: copy.start()
    finish = lambda copy: copy.wait_send()
    nothing = lambda b: None
    tok_ways, w_ways = 1 + nx, 1 + nc
    pieces = 2 + chunks

    def tok_forward(step, act, arrive):
        each_forward(
            lambda b, way: tok_copy(b, way), None, z, nz - 1, tok_ways, step, act, arrive
        )

    def w_forward(k, step, act, arrive):
        each_forward(
            lambda b, way: w_copy(k, b, way), None, y, ny - 1, w_ways, step, act, arrive
        )

    def w_gathered(k):
        for step in range(1, ny):
            w_forward(k, step, start, lambda b: w_wait(k, b * nc + c))

    def w_across(k):
        for j in range(1, nc):
            for by in range(ny):
                w_wait(k, by * nc + (c + j) % nc)

    for k in range(pieces):
        for refs in w_parts(k):
            each_own(lambda way: w_copy(k, y, way, refs), y, ny - 1, w_ways, start)
    whole_down = own_parts(down_ref, s_down_ref, wd.at[tp])
    for n, parts in enumerate((w_parts(0), w_parts(1), whole_down)):
        for src, dst in parts:
            pltpu.make_async_copy(src, dst, local_sem.at[n]).start()

    for p in range(nc):
        pl.when(c == p)(lambda: side_own(p).start())

    values = tokens_ref[...].astype(jnp.float32)
    scale_inv = lax.rsqrt(jnp.mean(values * values, axis=-1, keepdims=True) + norm_eps)
    normed = (values * scale_inv * gain_ref[...]).astype(jnp.bfloat16)
    mine = tok_rows(z, x)
    tok[mine, :width] = normed
    gated = normed.astype(jnp.float32) * side_gate_ref[...].astype(jnp.float32)
    opening = 1.0 / (1.0 + jnp.exp(-jnp.sum(gated, axis=-1, keepdims=True)))
    lane = lax.broadcasted_iota(jnp.int32, (rows, 128), 1)
    first = lane % 64
    aux = jnp.where(first == experts_all, opening, 0.0)
    for k in range(ids_ref.shape[1]):
        aux = aux + jnp.where(first == ids_ref[:, k : k + 1], route_ref[:, k : k + 1], 0.0)
    high = aux.astype(jnp.bfloat16)
    low = (aux - high.astype(jnp.float32)).astype(jnp.bfloat16)
    tok[mine, width:] = jnp.where(
        lane < 64, high.astype(jnp.float32), low.astype(jnp.float32)
    ).astype(jnp.bfloat16)
    each_own(lambda way: tok_copy(z, way), z, nz - 1, tok_ways, start)

    def arrive_tok(b):
        tok_wait(b, x)

    for step in range(1, nz):
        tok_forward(step, start, arrive_tok)
        if step == 1:
            side_each(start)
        if step == nz - 2:
            w_gathered(0)
    w_gathered(1)
    w_across(0)
    w_across(1)
    for n, place in enumerate((wg, wu, wd)):
        pltpu.make_async_copy(place.at[tp], place.at[tp], local_sem.at[n]).wait()

    tile = 2 * rows

    def column(at, n):
        aux = tok[at, width:].astype(jnp.float32)
        lane = lax.broadcasted_iota(jnp.int32, aux.shape, 1)
        hit = jnp.logical_or(lane == n, lane == n + 64)
        return jnp.sum(jnp.where(hit, aux, 0.0), axis=1, keepdims=True)

    for j in range(nx):
        bx = (x + j) % nx

        def hidden_tile(i, carry):
            pair = (z // 2 + i) % (nz // 2)
            if j:
                tok_wait(2 * pair, bx)
                tok_wait(2 * pair + 1, bx)
            at = pl.ds(pl.multiple_of(bx * nz * rows + pair * tile, rows), tile)
            a = tok[at, :width]
            gate_part = lax.dot_general(
                a, wg[...].reshape(n_tp * part, width), NT, preferred_element_type=jnp.float32
            )
            up_part = lax.dot_general(
                a, wu[...].reshape(n_tp * part, width), NT, preferred_element_type=jnp.float32
            )
            scale = mask_ref[local_experts : local_experts + 1, :]
            for e in range(local_experts):
                scale = scale + column(at, me * local_experts + e) * mask_ref[e : e + 1, :]
            hidden[at] = (silu(gate_part) * up_part * scale).astype(jnp.bfloat16)
            return carry

        lax.fori_loop(0, nz // 2, hidden_tile, 0)
        if j == 0:
            for p in range(nc):
                pl.when(c == p)(lambda: side_own(p).wait())
            for d in range(1, n_ep):
                at = (me + d) % n_ep
                block = side.at[c * n_ep + at]
                pltpu.make_async_remote_copy(
                    src_ref=block, dst_ref=block, send_sem=side_send.at[0],
                    recv_sem=side_recv.at[at], device_id=(me, tp), device_id_type=MESH,
                ).wait_recv()
            swap_copy().start()

    other = side.at[pl.ds((1 - c) * n_ep, n_ep)]
    pltpu.make_async_remote_copy(
        src_ref=other, dst_ref=other, send_sem=swap_send, recv_sem=swap_recv,
        device_id=(me, tp), device_id_type=MESH,
    ).wait_recv()

    def side_tile(i, carry):
        at = pl.ds(pl.multiple_of(i * tile, rows), tile)
        side_part = jnp.dot(
            tok[at, :width], side[:n_ep].reshape(width, side_cols),
            preferred_element_type=jnp.float32,
        )
        side_hid[at] = (silu(side_part) * column(at, experts_all)).astype(jnp.bfloat16)
        return carry

    lax.fori_loop(0, n_ep * rows // tile, side_tile, 0)

    def x_copy(q, j, bz):
        block = pl.ds(pl.multiple_of(bz * rows, rows), rows)
        return pltpu.make_async_remote_copy(
            src_ref=xs.at[q, j - 1, block],
            dst_ref=xr.at[q, j - 1, block],
            send_sem=x_send.at[q, j - 1, bz],
            recv_sem=x_recv.at[q, j - 1, bz],
            device_id=(z * nx + (x + j) % nx, tp),
            device_id_type=MESH,
        )

    def r_copy(q, dz):
        return pltpu.make_async_remote_copy(
            src_ref=sent.at[q, dz], dst_ref=got.at[q, dz + 1], send_sem=r_send.at[q, dz],
            recv_sem=r_recv.at[q, dz], device_id=(me + nx, tp), device_id_type=MESH,
        )

    def l_copy(q, dz):
        return pltpu.make_async_remote_copy(
            src_ref=sent.at[q, dz], dst_ref=got.at[q, dz], send_sem=l_send.at[q, dz],
            recv_sem=l_recv.at[q, dz], device_id=(me - nx, tp), device_id_type=MESH,
        )

    blocks_per = piece // side_rows

    def multiply(q):
        down = wd[:, :, cols(q)].reshape(n_tp * part, piece)
        side_down = side[pl.ds(n_ep + q * blocks_per, blocks_per)].reshape(piece, side_cols)
        for j in list(range(1, nx)) + [0]:
            at = pl.ds(pl.multiple_of((x + j) % nx * nz * rows, rows), nz * rows)
            value = jnp.dot(hidden[at], down, preferred_element_type=jnp.float32)
            value = value + lax.dot_general(
                side_hid[at], side_down, NT, preferred_element_type=jnp.float32
            )
            if j:
                xs[q, j - 1] = value.astype(jnp.bfloat16)
                for k in range(nz):
                    far = (1 - z * 2 // nz) * (nz - 1 - k) + z * 2 // nz * k
                    x_copy(q, j, far).start()
            else:
                acc[q] = value

    def reduce(q):
        def own(dz):
            block = pl.ds(pl.multiple_of(dz * rows, rows), rows)
            value = acc[q, block]
            for j in range(1, nx):
                x_copy(q, j, dz).wait_recv()
                value = value + xr[q, j - 1, block].astype(jnp.float32)
            return value

        def right(dz):
            value = own(dz)

            @pl.when(z == 0)
            def _():
                sent[q, dz] = value.astype(jnp.bfloat16)

            @pl.when(z > 0)
            def _():
                r_copy(q, dz).wait_recv()
                sent[q, dz] = (value + got[q, dz + 1].astype(jnp.float32)).astype(jnp.bfloat16)

            r_copy(q, dz).start()

        def left(dz):
            value = own(dz)

            @pl.when(z == nz - 1)
            def _():
                sent[q, dz] = value.astype(jnp.bfloat16)

            @pl.when(z < nz - 1)
            def _():
                l_copy(q, dz).wait_recv()
                sent[q, dz] = (value + got[q, dz].astype(jnp.float32)).astype(jnp.bfloat16)

            l_copy(q, dz).start()

        @pl.when(z * 2 < nz)
        def _():
            for k in range(nz - 1):
                pl.when(z < nz - 1 - k)(functools.partial(right, nz - 1 - k))
                pl.when(z > k)(functools.partial(left, k))

        @pl.when(z * 2 >= nz)
        def _():
            for k in range(nz - 1):
                pl.when(z > k)(functools.partial(left, k))
                pl.when(z < nz - 1 - k)(functools.partial(right, nz - 1 - k))

        acc[q, pl.ds(0, rows)] = own(z)

    def settle(q):
        @pl.when(z > 0)
        def _():
            r_copy(q, z).wait_recv()
            acc[q, pl.ds(0, rows)] += got[q, z + 1].astype(jnp.float32)

        @pl.when(z < nz - 1)
        def _():
            l_copy(q, z).wait_recv()
            acc[q, pl.ds(0, rows)] += got[q, z].astype(jnp.float32)

        out_ref[:, cols(q)] = acc[q, pl.ds(0, rows)].astype(jnp.bfloat16)

    for q in range(chunks):
        w_gathered(2 + q)
        w_across(2 + q)
        multiply(q)
        if q:
            reduce(q - 1)
    reduce(chunks - 1)
    for q in range(chunks):
        settle(q)

    each_own(lambda way: tok_copy(z, way), z, nz - 1, tok_ways, finish)
    for step in range(1, nz):
        tok_forward(step, finish, nothing)
    for k in range(pieces):
        each_own(lambda way: w_copy(k, y, way), y, ny - 1, w_ways, finish)
        for step in range(1, ny):
            w_forward(k, step, finish, nothing)
    side_each(finish)
    swap_copy().wait_send()
    for q in range(chunks):
        for j in range(1, nx):
            for bz in range(nz):
                x_copy(q, j, bz).wait_send()
        for dz in range(nz):
            pl.when(z < dz)(lambda: r_copy(q, dz).wait_send())
            pl.when(z > dz)(lambda: l_copy(q, dz).wait_send())


def body(
    nx,
    nc,
    tokens,
    norm_gain,
    expert_ids,
    route_weights,
    expert_gate,
    expert_up,
    expert_down,
    shared_gate,
    shared_up,
    shared_down,
    side_in,
    side_out,
    side_gate,
):
    tok_count, width = tokens.shape
    n_ep, n_tp = lax.axis_size("ep"), lax.axis_size("tp")
    nz, ny = n_ep // nx, n_tp // nc
    me = lax.axis_index("ep")
    local_experts, ff_part, _ = expert_gate.shape
    routed = local_experts * ff_part
    experts_all = n_ep * local_experts
    shared_rows = shared_gate.shape[0] // n_ep
    side_rows, side_all = side_in.shape
    side_cols = side_all // n_ep
    chunks = 8
    piece = width // chunks
    part = routed + -(-shared_rows // 16) * 16

    def shared_part(array):
        if shared_rows % 16 == 0:
            return array
        own = lax.dynamic_slice_in_dim(array, me * shared_rows, shared_rows, 0)
        return jnp.pad(own, ((0, part - routed - shared_rows), (0, 0)))

    def side_part(array):
        if side_cols % 128 == 0:
            return array
        return array.reshape(side_rows, n_ep, side_cols).transpose(1, 0, 2)

    place = np.minimum(np.arange(n_tp * part) % part // ff_part, local_experts)
    mask = (place[None, :] == np.arange(local_experts + 1)[:, None]).astype(np.float32)

    bf16, f32 = jnp.bfloat16, jnp.float32
    dma = pltpu.SemaphoreType.DMA
    dims = (nz, nx, ny, nc, experts_all, local_experts, chunks)
    return pl.pallas_call(
        functools.partial(kernel, dims),
        out_shape=jax.ShapeDtypeStruct((tok_count, width), bf16),
        in_specs=[pl.BlockSpec(memory_space=pltpu.VMEM)] * 6
        + [pl.BlockSpec(memory_space=pl.ANY)] * 8,
        out_specs=pl.BlockSpec(memory_space=pltpu.VMEM),
        scratch_shapes=[
            pltpu.VMEM((n_ep * tok_count, width + 128), bf16),
            pltpu.VMEM((n_tp, part, width), bf16),
            pltpu.VMEM((n_tp, part, width), bf16),
            pltpu.VMEM((n_tp, part, width), bf16),
            pltpu.VMEM((2 * n_ep, side_rows, side_cols), bf16),
            pltpu.VMEM((n_ep * tok_count, n_tp * part), bf16),
            pltpu.VMEM((n_ep * tok_count, side_cols), bf16),
            pltpu.VMEM((chunks, nz * tok_count, piece), f32),
            pltpu.VMEM((chunks, nx - 1, nz * tok_count, piece), bf16),
            pltpu.VMEM((chunks, nx - 1, nz * tok_count, piece), bf16),
            pltpu.VMEM((chunks, nz, tok_count, piece), bf16),
            pltpu.VMEM((chunks, nz + 1, tok_count, piece), bf16),
            dma((nz, 1 + nx)),
            dma((n_ep,)),
            dma((2 + chunks, ny, 1 + nc)),
            dma((2 + chunks, n_tp)),
            dma((n_ep,)),
            dma((n_ep,)),
            dma,
            dma,
            dma((4,)),
            dma((chunks, nx - 1, nz)),
            dma((chunks, nx - 1, nz)),
            dma((chunks, nz)),
            dma((chunks, nz)),
            dma((chunks, nz)),
            dma((chunks, nz)),
        ],
        compiler_params=pltpu.CompilerParams(
            collective_id=0, has_side_effects=True, vmem_limit_bytes=63000 * 1024
        ),
        name="layer",
    )(
        tokens, norm_gain[None, :], expert_ids, route_weights, side_gate[None, :], mask,
        expert_gate.reshape(routed, width), expert_up.reshape(routed, width),
        expert_down.reshape(routed, width), shared_part(shared_gate), shared_part(shared_up),
        shared_part(shared_down), side_part(side_in), side_part(side_out),
    )


def solution(mesh):
    devices = mesh.devices
    nx = len({d.coords[0] for d in devices[:, 0]})
    nc = len({d.core_on_chip for d in devices[0, :]})
    placed = (
        P(("ep", "tp"), None),
        P(),
        P(("ep", "tp"), None),
        P(("ep", "tp"), None),
        P("ep", "tp", None),
        P("ep", "tp", None),
        P("ep", "tp", None),
        P("tp", None),
        P("tp", None),
        P("tp", None),
        P("ep", None),
        P("ep", None),
        P(),
    )
    return jax.shard_map(
        functools.partial(body, nx, nc),
        mesh=mesh,
        in_specs=placed,
        out_specs=P(("ep", "tp"), None),
        check_vma=False,
    )
```

profile of v0, /device:TPU:0, one launch (start us, length us, event | category | flops | bytes accessed | tf_op | source)
XLA Modules:
  0.0 150.8 jit_solution(10107020644007738608)
XLA Ops:
  0.0 0.0 copy-start.2
  0.0 0.0 copy-start
  0.0 0.7 copy-done.2
  0.7 0.6 broadcast_in_dim.7.side_gate_ref
  1.3 0.0 copy-done
  1.3 0.0 copy-start.1
  1.3 0.7 copy.15.ids_ref
  2.0 0.0 copy-done.1
  2.0 0.7 copy.16.route_ref
  2.8 146.1 %layer.1 = bf16[144,2048]{1,0:T(8,128)(2,1)} custom-call(bf16[144,2048]{1,0:T(8,128)(2,1)} %tokens_ref.1, f32[1,2048]{1,0:T(1,128)} %bitcast.7, s32[144,8]{1,0:T(8,128)} %copy.15.ids_ref, f32[144,8]{1,0:T(8,128)} %copy.16.route_ref, bf16[1,2048]{1,0:T(2,128)(2,1)} %broadcast_in_dim.7.side_gate_ref, f32[3,1088]{1,0:T(4,128)} %constant.2.clone.mask_ref, ...), custom_call_target="tpu_custom_call" | custom-call | tf_op jit(solution)/shard_map/layer/pallas_call | solution.py:509
  148.8 1.9 %copy.18 = bf16[144,2048]{1,0:T(8,128)(2,1)} copy(bf16[144,2048]{1,0:T(8,128)(2,1)} %layer.1) | data formatting | bytes 1179648
Async XLA Ops:
  0.0 0.7 copy-start.2
  0.0 1.3 copy-start
  1.3 0.7 copy-start.1
where the time goes:
time: 151 us
  Pallas kernels  146 us (97%)
  local copies, waits for them, and re-layouts  4.68 us (3%)
    pallas_call x1, Pallas kernels, body(): pl.pallas_call(functools.partial(kernel, dims), out_shape=jax.ShapeDtypeS...  146 us
    unnamed x9, local copies, waits for them, and re-layouts  4.09 us

commit v1 on v0

v1 whole, which is shorter than its diff:
```python
import functools

import jax
import jax.numpy as jnp
from jax import lax
from jax.experimental import pallas as pl
from jax.experimental.pallas import tpu as pltpu
from jax.sharding import PartitionSpec as P

norm_eps = 1.0
MESH = pl.DeviceIdType.MESH
NT = (((1,), (1,)), ((), ()))


def silu(v):
    return v / (1.0 + jnp.exp(-v))


def when(conds, act):
    conds = [cond() for cond in conds]
    if any(cond is False for cond in conds):
        return
    conds = [cond for cond in conds if cond is not True]
    if not conds:
        act()
        return
    both = conds[0]
    for cond in conds[1:]:
        both = jnp.logical_and(both, cond)
    pl.when(both)(act)


def kernel(
    dims,
    tokens_ref, gain_ref, ids_ref, route_ref, side_gate_ref,
    gate_ref, up_ref, down_ref, s_gate_ref, s_up_ref, s_down_ref, side_in_ref, side_out_ref,
    out_ref,
    tok, wall, side, hidden, side_hid, acc, xs, xr, sent, got, hgot, saux, sc, scol,
    tok_send, tok_recv, hyb_send, w_send, w_recv, side_send, side_recv, swap_send, swap_recv,
    local_sem, aux_send, aux_recv, x_send, x_recv, r_send, l_send, z_recv, h_send, h_recv,
):
    nz, nx, ny, nc, local_experts, pieces, extra, chunks, ahead = dims
    n_ep, n_tp = nz * nx, ny * nc
    me, tp = lax.axis_index("ep"), lax.axis_index("tp")
    z, x = me // nx, me % nx
    y, c = tp // nc, tp % nc
    rows, width = tokens_ref.shape
    routed = gate_ref.shape[0]
    pr = routed // pieces
    per_expert = pieces // local_experts
    piece_units, shared_units = n_tp * pr, n_tp * extra
    side_rows, side_cols = side.shape[1:]
    piece = width // chunks
    half_w = width // 2
    down_at = 2 * (routed + extra)
    tile = 2 * rows
    hyb = nx == 2 and nz == 4
    tiles = n_ep // 2

    near = [
        sorted(range(nz), key=lambda b: (abs(b - zz), -b if 2 * zz < nz else b))
        for zz in range(nz)
    ]
    place_of = [[near[zz].index(b) for b in range(nz)] for zz in range(nz)]

    def by_z(values):
        out = values[0]
        if all(v == out for v in values):
            return out
        for zz in range(1, nz):
            out = jnp.where(z == zz, values[zz], out)
        return out

    def flag(values):
        values = [bool(v) for v in values]
        if all(values) or not any(values):
            return values[0]
        return by_z([int(v) for v in values]) == 1

    ends = lambda: flag([zz in (0, nz - 1) for zz in range(nz)])
    inner = lambda: flag([zz not in (0, nz - 1) for zz in range(nz)])
    twin = z + 1 - 2 * (z % 2)

    def slot(j, k):
        return k // 2 * (2 * nx) + 2 * j + k % 2

    def cols(q):
        return pl.ds(q * piece, piece)

    barrier = pltpu.get_barrier_semaphore()
    for j in range(1, n_ep):
        pl.semaphore_signal(barrier, inc=1, device_id=((me + j) % n_ep, tp), device_id_type=MESH)
    for j in range(1, n_tp):
        pl.semaphore_signal(barrier, inc=1, device_id=(me, (tp + j) % n_tp), device_id_type=MESH)


    def slot_rows(s):
        return pl.ds(s * rows if isinstance(s, int) else pl.multiple_of(s * rows, 16), rows)

    def tok_copy(from_slot, to_slot, h, target, send):
        part = pl.ds(h * half_w, half_w)
        return pltpu.make_async_remote_copy(
            src_ref=tok.at[slot_rows(from_slot), part],
            dst_ref=tok.at[slot_rows(to_slot), part],
            send_sem=send, recv_sem=tok_recv.at[to_slot, h],
            device_id=target, device_id_type=MESH,
        )

    def tok_wait(s, h):
        tok_copy(s, s, h, (me, tp), tok_send.at[0, 0, 0]).wait_recv()

    def along(k, h, d):
        to = by_z([
            place_of[zz + d][near[zz][k]] if 0 <= zz + d < nz else 0 for zz in range(nz)
        ])
        return tok_copy(
            slot(0, k), slot(0, to), h, (me + d * nx, tp), tok_send.at[k, (1 - d) // 2, h]
        )

    def across(k, h, j):
        return tok_copy(
            slot(0, k), slot(nx - j, k), h, (z * nx + (x + j) % nx, tp), tok_send.at[k, 1 + j, h]
        )

    def onward(k, to, h):
        return tok_copy(
            slot(1, k), slot(1, to), h, (me + (twin - z) * nx, tp), hyb_send.at[h]
        )

    def crosses(k, h):
        if hyb and k == nz - 1 and h == 1:
            return inner
        if hyb and k == nz - 2:
            return ends
        return lambda: True

    log = []

    def launch(conds, copy):
        log.append((conds, copy))
        when(conds, lambda: copy().start())

    def send_block(conds, k, h):
        bind = functools.partial
        for d in (1, -1):
            goes = [
                0 <= zz + d < nz and (near[zz][k] - zz) * d <= 0 for zz in range(nz)
            ]
            launch(conds + [lambda goes=goes: flag(goes)], bind(along, k, h, d))
        for j in range(1, nx):
            launch(conds + [crosses(k, h)], bind(across, k, h, j))

    def stage(step, h):
        for k in range(1, nz):
            here = [abs(near[zz][k] - zz) == step for zz in range(nz)]
            if any(here):
                cond = lambda here=here: flag(here)
                when([cond], lambda: tok_wait(slot(0, k), h))
                send_block([cond], k, h)
        if hyb and step == 1:
            tok_wait(slot(1, 0), h)
            launch([ends], functools.partial(onward, 0, nz - 2, h))
        if hyb and step == nz - 1 and h == 1:
            when([inner], lambda: tok_wait(slot(1, nz - 1), 1))
            launch([inner], functools.partial(onward, nz - 1, nz - 1, 1))

    def cross_wait(half):
        for j in range(1, nx):
            for k in (2 * half, 2 * half + 1):
                for h in range(2):
                    if hyb and k == 0:
                        continue
                    conds = [ends] if hyb and k == nz - 1 and h == 1 else []
                    when(conds, lambda: tok_wait(slot(j, k), h))


    shared_at = pl.ds(0, extra)
    if s_gate_ref.shape[0] > extra:
        shared_at = pl.ds(pl.multiple_of(me * extra, extra), extra)

    def w_parts(k):
        slab = wall.at[tp]
        if k < pieces:
            at, r0 = pl.ds(k * pr, pr), 2 * extra + 2 * k * pr
            parts = [
                (gate_ref.at[at], slab.at[pl.ds(r0, pr)]),
                (up_ref.at[at], slab.at[pl.ds(r0 + pr, pr)]),
            ]
            if k == 0:
                parts += [
                    (s_gate_ref.at[shared_at], slab.at[pl.ds(0, extra)]),
                    (s_up_ref.at[shared_at], slab.at[pl.ds(extra, extra)]),
                ]
            return parts
        q = cols(k - pieces)
        return [
            (down_ref.at[:, q], slab.at[pl.ds(down_at, routed), q]),
            (s_down_ref.at[shared_at, q], slab.at[pl.ds(down_at + routed, extra), q]),
        ]

    def w_place(k, owner):
        if k == 0:
            return wall.at[owner, pl.ds(0, 2 * (extra + pr))]
        if k < pieces:
            return wall.at[owner, pl.ds(2 * (extra + k * pr), 2 * pr)]
        return wall.at[owner, pl.ds(down_at, routed + extra), cols(k - pieces)]

    def w_copy(k, by, way, refs=None):
        if way < 2:
            target = (me, tp + nc if way == 0 else tp - nc)
        else:
            target = (me, y * nc + (c + way - 1) % nc)
        owner = by * nc + c
        if refs is None:
            refs = (wall.at[owner],) * 2 if k is None else (w_place(k, owner),) * 2
        return pltpu.make_async_remote_copy(
            src_ref=refs[0], dst_ref=refs[1], send_sem=w_send.at[by, way],
            recv_sem=w_recv.at[0 if k is None else k, owner],
            device_id=target, device_id_type=MESH,
        )

    def w_wait(k, owner):
        pltpu.make_async_remote_copy(
            src_ref=w_place(k, owner), dst_ref=w_place(k, owner), send_sem=w_send.at[0, 0],
            recv_sem=w_recv.at[k, owner], device_id=(me, tp), device_id_type=MESH,
        ).wait_recv()

    def each_own(copy_of, act):
        pl.when(y < ny - 1)(lambda: act(copy_of(0)))
        pl.when(y > 0)(lambda: act(copy_of(1)))
        for way in range(2, 1 + nc):
            act(copy_of(way))

    def each_forward(copy_of, step, act, arrive):
        @pl.when(y >= step)
        def _():
            b = y - step
            arrive(b)
            pl.when(y < ny - 1)(lambda: act(copy_of(b, 0)))
            for way in range(2, 1 + nc):
                act(copy_of(b, way))

        @pl.when(y + step <= ny - 1)
        def _():
            b = y + step
            arrive(b)
            pl.when(y > 0)(lambda: act(copy_of(b, 1)))
            for way in range(2, 1 + nc):
                act(copy_of(b, way))

    start = lambda copy: copy.start()
    finish = lambda copy: copy.wait_send()

    def w_gathered(k):
        for step in range(1, ny):
            each_forward(
                lambda b, way: w_copy(k, b, way), step, start, lambda b: w_wait(k, b * nc + c)
            )

    def w_across(k):
        for j in range(1, nc):
            for by in range(ny):
                w_wait(k, by * nc + (c + j) % nc)


    def side_source(ref, to):
        if len(ref.shape) == 3:
            return ref.at[to]
        return ref.at[:, pl.ds(pl.multiple_of(to * side_cols, side_cols), side_cols)]

    def side_copy(j, p):
        to = (me + j) % n_ep
        return pltpu.make_async_remote_copy(
            src_ref=side_source((side_in_ref, side_out_ref)[p], to),
            dst_ref=side.at[p * n_ep + me],
            send_sem=side_send, recv_sem=side_recv, device_id=(to, tp), device_id_type=MESH,
        )

    def side_all():
        whole = side.at[pl.ds(0, n_ep - 1)]
        return pltpu.make_async_remote_copy(
            src_ref=whole, dst_ref=whole, send_sem=side_send, recv_sem=side_recv,
            device_id=(me, tp), device_id_type=MESH,
        )

    def side_own(p):
        return pltpu.make_async_copy(
            side_source((side_in_ref, side_out_ref)[p], me), side.at[p * n_ep + me],
            local_sem.at[1],
        )

    def swap_copy(half):
        part = side.at[pl.ds(half * n_ep, n_ep)]
        return pltpu.make_async_remote_copy(
            src_ref=part, dst_ref=part, send_sem=swap_send, recv_sem=swap_recv,
            device_id=(me, y * nc + 1 - c), device_id_type=MESH,
        )


    def aux_copy(k, j):
        to = by_z([near[zz][k] for zz in range(nz)]) * nx + (x + j) % nx
        k_there = by_z([place_of[near[zz][k]][zz] for zz in range(nz)])
        return pltpu.make_async_remote_copy(
            src_ref=saux.at[to], dst_ref=sc.at[slot((nx - j) % nx, k_there)],
            send_sem=aux_send, recv_sem=aux_recv, device_id=(to, tp), device_id_type=MESH,
        )

    def aux_all():
        return pltpu.make_async_remote_copy(
            src_ref=saux.at[pl.ds(0, n_ep - 1)], dst_ref=sc.at[pl.ds(0, n_ep - 1)],
            send_sem=aux_send, recv_sem=aux_recv, device_id=(me, tp), device_id_type=MESH,
        )

    for k in range(pieces + chunks):
        for part in w_parts(k):
            pltpu.make_async_copy(*part, local_sem.at[0]).start()
    for p in range(nc):
        pl.when(c == p)(lambda: side_own(p).start())

    values = tokens_ref[...].astype(jnp.float32)
    scale_inv = lax.rsqrt(jnp.mean(values * values, axis=-1, keepdims=True) + norm_eps)
    normed = (values * scale_inv * gain_ref[...]).astype(jnp.bfloat16)
    tok[slot_rows(0), :] = normed

    pl.semaphore_wait(barrier, n_ep + n_tp - 2)
    for h in range(2):
        send_block([], 0, h)
    for k in range(pieces + chunks):
        for refs in w_parts(k):
            each_own(lambda way: w_copy(k, y, way, refs), start)

    side_vector = side_gate_ref[...].astype(jnp.float32)
    lanes = side_vector.shape[1]
    side_vector = jnp.concatenate(
        [jnp.broadcast_to(side_vector[i : i + 1], (8, lanes)) for i in range(width // lanes)],
        axis=1,
    ).astype(jnp.bfloat16)
    opening = lax.dot_general(side_vector, normed, NT, preferred_element_type=jnp.float32)
    opening = 1.0 / (1.0 + jnp.exp(-opening))
    ids, route = ids_ref[...], route_ref[...]
    row = lax.broadcasted_iota(jnp.int32, (8, rows), 0)
    for to in range(n_ep):
        block = jnp.where(row == local_experts, opening, 0.0)
        for e in range(local_experts):
            hit = jnp.where(ids == to * local_experts + e, route, 0.0)
            block = jnp.where(row == e, jnp.sum(hit, axis=0, keepdims=True), block)
        gap = sc.shape[2] - rows
        saux[to] = jnp.concatenate([block, jnp.zeros((8, gap), jnp.float32)], axis=1)
    sc[0] = saux[me]
    for k in range(nz):
        for j in range(nx):
            if k or j:
                aux_copy(k, j).start()


    def tile_rows(t):
        return pl.ds(pl.multiple_of(t * tile, 16), tile)

    def column(at, n):
        picked = scol[at, :]
        lane = lax.broadcasted_iota(jnp.int32, picked.shape, 1)
        return jnp.sum(jnp.where(lane == n, picked, 0.0), axis=1, keepdims=True)

    def nt(a, b):
        return lax.dot_general(a, b, NT, preferred_element_type=jnp.float32)

    def unit(t, p):
        at = tile_rows(t)
        r0 = 2 * extra + p * (2 * pr)
        if not isinstance(p, int):
            r0 = pl.multiple_of(r0, 16)
        a = tok[at, :]
        gate = wall[:, pl.ds(r0, pr), :].reshape(piece_units, width)
        up = wall[:, pl.ds(r0 + pr, pr), :].reshape(piece_units, width)
        gated = silu(nt(a, gate)) * nt(a, up) * column(at, p // per_expert)
        to = p * piece_units if isinstance(p, int) else pl.multiple_of(p * piece_units, 128)
        hidden[at, pl.ds(to, piece_units)] = gated.astype(jnp.bfloat16)

    def units(t0, t1, p0, p1):
        n = p1 - p0
        if (t1 - t0) * n > 0:
            def step(i, carry):
                unit(t0 + i // n, p0 + i % n)
                return carry

            lax.fori_loop(0, (t1 - t0) * n, step, 0)

    def extras(t0, t1):
        def step(t, carry):
            at = tile_rows(t)
            a = tok[at, :]
            both = jnp.concatenate([
                wall[:, :extra, :].reshape(shared_units, width),
                wall[:, extra : 2 * extra, :].reshape(shared_units, width),
            ], axis=0)
            both = nt(a, both)
            gated = silu(both[:, :shared_units]) * both[:, shared_units:]
            hidden[at, pieces * piece_units :] = gated.astype(jnp.bfloat16)
            side_part = jnp.dot(
                a, side[:n_ep].reshape(width, side_cols), preferred_element_type=jnp.float32
            )
            side_hid[at] = (silu(side_part) * column(at, local_experts)).astype(jnp.bfloat16)
            return carry

        lax.fori_loop(t0, t1, step, 0)

    def arrive(k):
        w_gathered(k)
        w_across(k)

    for h in range(2):
        stage(1, h)
    for p in range(nc):
        def side_go(p=p):
            for j in range(1, n_ep):
                side_copy(j, p).start()

        pl.when(c == p)(side_go)
    pltpu.make_async_copy(wall.at[tp], wall.at[tp], local_sem.at[0]).wait()
    aux_all().wait_recv()
    for s in range(n_ep):
        scol[slot_rows(s), :] = sc[s].T[:rows]
    arrive(0)
    units(0, 1, 0, 1)
    stage(2, 0)
    arrive(1)
    units(0, 1, 1, 2)
    stage(2, 1)
    cross_wait(0)
    units(1, nx, 0, 2)
    for s in range(3, nz):
        stage(s, 0)
    for p in range(2, pieces - 1):
        arrive(p)
    units(0, nx, 2, pieces - 1)
    for s in range(3, nz):
        stage(s, 1)
    for p in range(nc):
        pl.when(c == p)(lambda: side_own(p).wait())
    side_all().wait_recv()
    swap_copy(c).start()
    units(nx, nx + 1, 0, pieces - 1)
    swap_copy(1 - c).wait_recv()
    extras(0, nx + 1)
    for half in range(1, nz // 2):
        cross_wait(half)
    units(nx + 1, tiles, 0, pieces - 1)
    arrive(pieces - 1)
    units(0, tiles, pieces - 1, pieces)
    extras(nx + 1, tiles)


    def x_index(j, k, q):
        return ((j - 1) * nz + k) * chunks + q

    def x_copy(q, j, k):
        i = x_index(j, k, q)
        return pltpu.make_async_remote_copy(
            src_ref=xs.at[i], dst_ref=xr.at[i], send_sem=x_send, recv_sem=x_recv.at[i],
            device_id=(z * nx + (x + j) % nx, tp), device_id_type=MESH,
        )

    def x_total(n):
        return pltpu.make_async_remote_copy(
            src_ref=xs.at[pl.ds(0, n)], dst_ref=xr.at[pl.ds(0, n)], send_sem=x_send,
            recv_sem=x_recv.at[0], device_id=(me, tp), device_id_type=MESH,
        )

    def h_copy(k, q):
        return pltpu.make_async_remote_copy(
            src_ref=xs.at[x_index(1, k, q)], dst_ref=hgot.at[q], send_sem=h_send,
            recv_sem=h_recv.at[q], device_id=(me + (twin - z) * nx, tp), device_id_type=MESH,
        )

    def h_total(n):
        return pltpu.make_async_remote_copy(
            src_ref=xs.at[pl.ds(0, n)], dst_ref=hgot.at[pl.ds(0, n)], send_sem=h_send,
            recv_sem=h_recv.at[0], device_id=(me, tp), device_id_type=MESH,
        )

    def z_copy(q, dz, right):
        return pltpu.make_async_remote_copy(
            src_ref=sent.at[dz * chunks + q], dst_ref=got.at[(dz + right) * chunks + q],
            send_sem=r_send if right else l_send, recv_sem=z_recv.at[(dz + right) * chunks + q],
            device_id=(me + nx if right else me - nx, tp), device_id_type=MESH,
        )

    def z_total(n, right):
        return pltpu.make_async_remote_copy(
            src_ref=sent.at[pl.ds(0, n)], dst_ref=got.at[pl.ds(0, n)],
            send_sem=r_send if right else l_send, recv_sem=z_recv.at[0],
            device_id=(me, tp), device_id_type=MESH,
        )

    blocks_per = piece // side_rows

    def multiply(q):
        down = jnp.concatenate(
            [
                wall[:, down_at + p * pr : down_at + (p + 1) * pr, cols(q)].reshape(
                    piece_units, piece
                )
                for p in range(pieces)
            ]
            + [wall[:, down_at + routed :, cols(q)].reshape(shared_units, piece)],
            axis=0,
        )
        side_down = side[pl.ds(n_ep + q * blocks_per, blocks_per)].reshape(piece, side_cols)

        def product(j, half):
            at = tile_rows(half * nx + j)
            return jnp.dot(hidden[at], down, preferred_element_type=jnp.float32) + nt(
                side_hid[at], side_down
            )

        def leave(j, k):
            go = lambda: x_copy(q, j, k).start()
            over = lambda: h_copy(k, q).start()
            if hyb and k == 3 and q % 2:
                when([ends], over)
            elif hyb and k == 2:
                when([ends], go)
                when([inner], over)
            elif hyb and k == 0:
                when([inner], go)
            else:
                go()

        for half in reversed(range(nz // 2)):
            for j in range(1, nx):
                value = product(j, half).astype(jnp.bfloat16)
                for i in (1, 0):
                    k = 2 * half + i
                    xs[x_index(j, k, q)] = value[i * rows : (i + 1) * rows]
                    leave(j, k)
        for half in reversed(range(nz // 2)):
            value = product(0, half)
            for i in range(2):
                acc[(2 * half + i) * chunks + q] = value[i * rows : (i + 1) * rows]

    def relay(q):
        def pass_on(k):
            h_copy(k, q).wait_recv()
            i = x_index(1, k, q)
            value = xs[i].astype(jnp.float32) + hgot[q].astype(jnp.float32)
            xs[i] = value.astype(jnp.bfloat16)
            x_copy(q, 1, k).start()

        if hyb:
            when([ends], lambda: pass_on(0))
            if q % 2:
                when([inner], lambda: pass_on(3))

    def fold(q, k):
        conds = []
        if hyb and k == 3 and q % 2:
            conds = [inner]
        if hyb and k == 2:
            conds = [ends]

        def add():
            value = acc[k * chunks + q]
            for j in range(1, nx):
                x_copy(q, j, k).wait_recv()
                value = value + xr[x_index(j, k, q)].astype(jnp.float32)
            acc[k * chunks + q] = value

        when(conds, add)

    def reduce(q):
        for k in range(nz - 1, 0, -1):
            fold(q, k)
            dz = by_z([near[zz][k] for zz in range(nz)])

            def move(right, far, k=k, dz=dz):
                def act():
                    value = acc[k * chunks + q]
                    mine = dz * chunks + q

                    @pl.when(z == far)
                    def _():
                        sent[mine] = value.astype(jnp.bfloat16)

                    @pl.when(z != far)
                    def _():
                        z_copy(q, dz, right).wait_recv()
                        more = got[(dz + right) * chunks + q].astype(jnp.float32)
                        sent[mine] = (value + more).astype(jnp.bfloat16)

                    z_copy(q, dz, right).start()

                return act

            when([lambda: flag([near[zz][k] > zz for zz in range(nz)])], move(1, 0))
            when([lambda: flag([near[zz][k] < zz for zz in range(nz)])], move(0, nz - 1))
        fold(q, 0)

    def settle(q):
        @pl.when(z > 0)
        def _():
            z_copy(q, z, 1).wait_recv()
            acc[q] += got[(z + 1) * chunks + q].astype(jnp.float32)

        @pl.when(z < nz - 1)
        def _():
            z_copy(q, z, 0).wait_recv()
            acc[q] += got[z * chunks + q].astype(jnp.float32)

        out_ref[:, cols(q)] = acc[q].astype(jnp.bfloat16)

    for i in range(chunks + ahead):
        if i < chunks:
            arrive(pieces + i)
            multiply(i)
        if 0 < i <= chunks:
            relay(i - 1)
        if i >= ahead:
            reduce(i - ahead)
    for q in range(chunks):
        settle(q)

    for conds, copy in log:
        when(conds, lambda: copy().wait_send())
    each_own(lambda way: w_copy(None, y, way), finish)
    for step in range(1, ny):
        each_forward(lambda b, way: w_copy(None, b, way), step, finish, lambda b: None)
    side_all().wait_send()
    swap_copy(c).wait_send()
    aux_all().wait_send()
    count = (nx - 1) * nz * chunks
    if hyb:
        when([ends], lambda: x_total(count - chunks // 2).wait_send())
        when([inner], lambda: x_total(count - chunks).wait_send())
        when([ends], lambda: h_total(chunks // 2).wait_send())
        when([inner], lambda: h_total(chunks).wait_send())
    else:
        x_total(count).wait_send()
    for zz in range(nz):
        if zz < nz - 1:
            pl.when(z == zz)(lambda: z_total((nz - 1 - zz) * chunks, 1).wait_send())
        if zz > 0:
            pl.when(z == zz)(lambda: z_total(zz * chunks, 0).wait_send())


def body(
    nx,
    nc,
    tokens,
    norm_gain,
    expert_ids,
    route_weights,
    expert_gate,
    expert_up,
    expert_down,
    shared_gate,
    shared_up,
    shared_down,
    side_in,
    side_out,
    side_gate,
):
    tok_count, width = tokens.shape
    n_ep, n_tp = lax.axis_size("ep"), lax.axis_size("tp")
    nz, ny = n_ep // nx, n_tp // nc
    me = lax.axis_index("ep")
    local_experts, ff_part, _ = expert_gate.shape
    routed = local_experts * ff_part
    shared_rows = shared_gate.shape[0] // n_ep
    side_rows, side_all = side_in.shape
    side_cols = side_all // n_ep
    chunks = 8
    ahead = 3
    pieces = 2 * local_experts
    piece = width // chunks
    extra = -(-shared_rows // 16) * 16
    padded = -(-tok_count // 128) * 128

    def shared_part(array):
        if shared_rows % 16 == 0:
            return array
        own = lax.dynamic_slice_in_dim(array, me * shared_rows, shared_rows, 0)
        return jnp.pad(own, ((0, extra - shared_rows), (0, 0)))

    def side_part(array):
        if side_cols % 128 == 0:
            return array
        return array.reshape(side_rows, n_ep, side_cols).transpose(1, 0, 2)

    bf16, f32 = jnp.bfloat16, jnp.float32
    dma = pltpu.SemaphoreType.DMA
    dims = (nz, nx, ny, nc, local_experts, pieces, extra, chunks, ahead)
    return pl.pallas_call(
        functools.partial(kernel, dims),
        out_shape=jax.ShapeDtypeStruct((tok_count, width), bf16),
        in_specs=[pl.BlockSpec(memory_space=pltpu.VMEM)] * 5
        + [pl.BlockSpec(memory_space=pl.ANY)] * 8,
        out_specs=pl.BlockSpec(memory_space=pltpu.VMEM),
        scratch_shapes=[
            pltpu.VMEM((n_ep * tok_count, width), bf16),
            pltpu.VMEM((n_tp, 3 * (routed + extra), width), bf16),
            pltpu.VMEM((2 * n_ep, side_rows, side_cols), bf16),
            pltpu.VMEM((n_ep * tok_count, n_tp * (routed + extra)), bf16),
            pltpu.VMEM((n_ep * tok_count, side_cols), bf16),
            pltpu.VMEM((nz * chunks, tok_count, piece), f32),
            pltpu.VMEM(((nx - 1) * nz * chunks, tok_count, piece), bf16),
            pltpu.VMEM(((nx - 1) * nz * chunks, tok_count, piece), bf16),
            pltpu.VMEM((nz * chunks, tok_count, piece), bf16),
            pltpu.VMEM(((nz + 1) * chunks, tok_count, piece), bf16),
            pltpu.VMEM((chunks if nx == 2 else 1, tok_count, piece), bf16),
            pltpu.VMEM((n_ep, 8, padded), f32),
            pltpu.VMEM((n_ep, 8, padded), f32),
            pltpu.VMEM((n_ep * tok_count, 8), f32),
            dma((nz, 1 + nx, 2)),
            dma((n_ep, 2)),
            dma((2,)),
            dma((ny, 1 + nc)),
            dma((pieces + chunks, n_tp)),
            dma,
            dma,
            dma,
            dma,
            dma((2,)),
            dma,
            dma,
            dma,
            dma(((nx - 1) * nz * chunks,)),
            dma,
            dma,
            dma(((nz + 1) * chunks,)),
            dma,
            dma((chunks,)),
        ],
        compiler_params=pltpu.CompilerParams(
            collective_id=0, has_side_effects=True, vmem_limit_bytes=63000 * 1024
        ),
        name="layer",
    )(
        tokens, norm_gain[None, :], expert_ids.T, route_weights.T, side_gate.reshape(-1, 128),
        expert_gate.reshape(routed, width), expert_up.reshape(routed, width),
        expert_down.reshape(routed, width), shared_part(shared_gate), shared_part(shared_up),
        shared_part(shared_down), side_part(side_in), side_part(side_out),
    )


def solution(mesh):
    devices = mesh.devices
    nx = len({d.coords[0] for d in devices[:, 0]})
    nc = len({d.core_on_chip for d in devices[0, :]})
    placed = (
        P(("ep", "tp"), None),
        P(),
        P(("ep", "tp"), None),
        P(("ep", "tp"), None),
        P("ep", "tp", None),
        P("ep", "tp", None),
        P("ep", "tp", None),
        P("tp", None),
        P("tp", None),
        P("tp", None),
        P("ep", None),
        P("ep", None),
        P(),
    )
    return jax.shard_map(
        functools.partial(body, nx, nc),
        mesh=mesh,
        in_specs=placed,
        out_specs=P(("ep", "tp"), None),
        check_vma=False,
    )
```

time: 151 us -> 140 us (0.927)
  Pallas kernels: 146 us -> 138 us
  local copies, waits for them, and re-layouts: 4.68 us -> 1.93 us
    pallas_call x1, Pallas kernels: 146 us -> 138 us  [body(): pl.pallas_call(functools.partial(kernel, dims), out_shape=jax.ShapeDtypeS...]
    unnamed x9 -> x1, local copies, waits for them, and re-layouts: 4.09 us -> 1.93 us
where the time goes in v1:
time: 140 us
  Pallas kernels  138 us (99%)
  local copies, waits for them, and re-layouts  1.93 us (1%)
    pallas_call x1, Pallas kernels, body(): pl.pallas_call(functools.partial(kernel, dims), out_shape=jax.ShapeDtypeS...  138 us

profile of v1, /device:TPU:0, one launch (start us, length us, event | category | flops | bytes accessed | tf_op | source)
XLA Modules:
  0.0 139.6 jit_solution(14659134816999011733)
XLA Ops:
  0.0 137.7 %layer.1 = bf16[144,2048]{1,0:T(8,128)(2,1)} custom-call(bf16[144,2048]{1,0:T(8,128)(2,1)} %tokens_ref.1, f32[1,2048]{1,0:T(1,128)} %bitcast.10, s32[8,144]{1,0:T(8,128)} %bitcast.11, f32[8,144]{1,0:T(8,128)} %bitcast.12, bf16[16,128]{1,0:T(8,128)(2,1)} %bitcast.13, bf16[256,2048]{1,0:T(8,128)(2,1)} %bitcast.7, bf16[256,2048]{1,0:T(8,128)(2,1)} %bitcast.8, ...), custom_call_target="tpu_custom_call" | custom-call | tf_op jit(solution)/shard_map/layer/pallas_call | solution.py:692
  137.7 1.9 %copy.15 = bf16[144,2048]{1,0:T(8,128)(2,1)} copy(bf16[144,2048]{1,0:T(8,128)(2,1)} %layer.1) | data formatting | bytes 1179648

commit v2 on v1

--- a/solution.py
+++ b/solution.py
@@ -39,7 +39,7 @@
     tok_send, tok_recv, hyb_send, w_send, w_recv, side_send, side_recv, swap_send, swap_recv,
     local_sem, aux_send, aux_recv, x_send, x_recv, r_send, l_send, z_recv, h_send, h_recv,
 ):
-    nz, nx, ny, nc, local_experts, pieces, extra, chunks, ahead = dims
+    nz, nx, ny, nc, local_experts, pieces, extra, chunks = dims
     n_ep, n_tp = nz * nx, ny * nc
     me, tp = lax.axis_index("ep"), lax.axis_index("tp")
     z, x = me // nx, me % nx
@@ -51,7 +51,9 @@
     piece_units, shared_units = n_tp * pr, n_tp * extra
     side_rows, side_cols = side.shape[1:]
     piece = width // chunks
-    half_w = width // 2
+    unit_w = width // 16
+    edges = [0, 5 * unit_w, 10 * unit_w, width]
+    parts = len(edges) - 1
     down_at = 2 * (routed + extra)
     tile = 2 * rows
     hyb = nx == 2 and nz == 4
@@ -98,7 +100,7 @@
         return pl.ds(s * rows if isinstance(s, int) else pl.multiple_of(s * rows, 16), rows)
 
     def tok_copy(from_slot, to_slot, h, target, send):
-        part = pl.ds(h * half_w, half_w)
+        part = pl.ds(edges[h], edges[h + 1] - edges[h])
         return pltpu.make_async_remote_copy(
             src_ref=tok.at[slot_rows(from_slot), part],
             dst_ref=tok.at[slot_rows(to_slot), part],
@@ -128,7 +130,7 @@
         )
 
     def crosses(k, h):
-        if hyb and k == nz - 1 and h == 1:
+        if hyb and k == nz - 1 and h == parts - 1:
             return inner
         if hyb and k == nz - 2:
             return ends
@@ -160,17 +162,17 @@
         if hyb and step == 1:
             tok_wait(slot(1, 0), h)
             launch([ends], functools.partial(onward, 0, nz - 2, h))
-        if hyb and step == nz - 1 and h == 1:
-            when([inner], lambda: tok_wait(slot(1, nz - 1), 1))
-            launch([inner], functools.partial(onward, nz - 1, nz - 1, 1))
+        if hyb and step == nz - 1 and h == parts - 1:
+            when([inner], lambda: tok_wait(slot(1, nz - 1), h))
+            launch([inner], functools.partial(onward, nz - 1, nz - 1, h))
 
     def cross_wait(half):
         for j in range(1, nx):
             for k in (2 * half, 2 * half + 1):
-                for h in range(2):
+                for h in range(parts):
                     if hyb and k == 0:
                         continue
-                    conds = [ends] if hyb and k == nz - 1 and h == 1 else []
+                    conds = [ends] if hyb and k == nz - 1 and h == parts - 1 else []
                     when(conds, lambda: tok_wait(slot(j, k), h))
 
 
@@ -323,7 +325,13 @@
     tok[slot_rows(0), :] = normed
 
     pl.semaphore_wait(barrier, n_ep + n_tp - 2)
-    for h in range(2):
+    for p in range(nc):
+        def side_go(p=p):
+            for j in range(1, n_ep):
+                side_copy(j, p).start()
+
+        pl.when(c == p)(side_go)
+    for h in range(parts):
         send_block([], 0, h)
     for k in range(pieces + chunks):
         for refs in w_parts(k):
@@ -404,50 +412,49 @@
 
         lax.fori_loop(t0, t1, step, 0)
 
-    def arrive(k):
-        w_gathered(k)
-        w_across(k)
-
-    for h in range(2):
+    for h in range(parts):
         stage(1, h)
-    for p in range(nc):
-        def side_go(p=p):
-            for j in range(1, n_ep):
-                side_copy(j, p).start()
-
-        pl.when(c == p)(side_go)
     pltpu.make_async_copy(wall.at[tp], wall.at[tp], local_sem.at[0]).wait()
+    w_gathered(0)
     aux_all().wait_recv()
     for s in range(n_ep):
         scol[slot_rows(s), :] = sc[s].T[:rows]
-    arrive(0)
+    w_across(0)
     units(0, 1, 0, 1)
-    stage(2, 0)
-    arrive(1)
+    for h in range(parts - 1):
+        stage(2, h)
+    w_gathered(1)
+    stage(2, parts - 1)
+    w_across(1)
     units(0, 1, 1, 2)
-    stage(2, 1)
     cross_wait(0)
     units(1, nx, 0, 2)
     for s in range(3, nz):
-        stage(s, 0)
+        for h in range(parts - 1):
+            stage(s, h)
     for p in range(2, pieces - 1):
-        arrive(p)
-    units(0, nx, 2, pieces - 1)
-    for s in range(3, nz):
-        stage(s, 1)
+        w_gathered(p)
     for p in range(nc):
         pl.when(c == p)(lambda: side_own(p).wait())
     side_all().wait_recv()
     swap_copy(c).start()
+    for p in range(2, pieces - 1):
+        w_across(p)
+    units(0, nx, 2, pieces - 1)
+    for s in range(3, nz):
+        stage(s, parts - 1)
     units(nx, nx + 1, 0, pieces - 1)
+    w_gathered(pieces - 1)
     swap_copy(1 - c).wait_recv()
     extras(0, nx + 1)
+    w_across(pieces - 1)
+    units(0, nx + 1, pieces - 1, pieces)
+    w_gathered(pieces)
     for half in range(1, nz // 2):
         cross_wait(half)
-    units(nx + 1, tiles, 0, pieces - 1)
-    arrive(pieces - 1)
-    units(0, tiles, pieces - 1, pieces)
-    extras(nx + 1, tiles)
+    units(nx + 1, tiles, 0, pieces)
+    w_gathered(pieces + 1)
+    w_across(pieces)
 
 
     def x_index(j, k, q):
@@ -494,7 +501,7 @@
 
     blocks_per = piece // side_rows
 
-    def multiply(q):
+    def product(q, j, half):
         down = jnp.concatenate(
             [
                 wall[:, down_at + p * pr : down_at + (p + 1) * pr, cols(q)].reshape(
@@ -506,37 +513,39 @@
             axis=0,
         )
         side_down = side[pl.ds(n_ep + q * blocks_per, blocks_per)].reshape(piece, side_cols)
-
-        def product(j, half):
-            at = tile_rows(half * nx + j)
-            return jnp.dot(hidden[at], down, preferred_element_type=jnp.float32) + nt(
-                side_hid[at], side_down
-            )
-
-        def leave(j, k):
-            go = lambda: x_copy(q, j, k).start()
-            over = lambda: h_copy(k, q).start()
-            if hyb and k == 3 and q % 2:
-                when([ends], over)
-            elif hyb and k == 2:
-                when([ends], go)
-                when([inner], over)
-            elif hyb and k == 0:
-                when([inner], go)
-            else:
-                go()
-
-        for half in reversed(range(nz // 2)):
-            for j in range(1, nx):
-                value = product(j, half).astype(jnp.bfloat16)
-                for i in (1, 0):
-                    k = 2 * half + i
-                    xs[x_index(j, k, q)] = value[i * rows : (i + 1) * rows]
-                    leave(j, k)
-        for half in reversed(range(nz // 2)):
-            value = product(0, half)
-            for i in range(2):
-                acc[(2 * half + i) * chunks + q] = value[i * rows : (i + 1) * rows]
+        at = tile_rows(half * nx + j)
+        return jnp.dot(hidden[at], down, preferred_element_type=jnp.float32) + nt(
+            side_hid[at], side_down
+        )
+
+    def detour(q, k):
+        return hyb and k == 3 and q < chunks // 2
+
+    def leave(q, j, k):
+        go = lambda: x_copy(q, j, k).start()
+        if detour(q, k):
+            when([ends], lambda: h_copy(k, q).start())
+        elif hyb and k == 2:
+            when([ends], go)
+        elif hyb and k == 0:
+            when([inner], go)
+        else:
+            go()
+
+    def partial_sum(q, half, j):
+        value = product(q, j, half).astype(jnp.bfloat16)
+        for i in (1, 0):
+            k = 2 * half + i
+            xs[x_index(j, k, q)] = value[i * rows : (i + 1) * rows]
+            if q < chunks // 2 or k == nz - 1:
+                leave(q, j, k)
+            if hyb and k == 2:
+                when([inner], lambda: h_copy(k, q).start())
+
+    def own_sum(q, half):
+        value = product(q, 0, half)
+        for i in range(2):
+            acc[(2 * half + i) * chunks + q] = value[i * rows : (i + 1) * rows]
 
     def relay(q):
         def pass_on(k):
@@ -548,12 +557,12 @@
 
         if hyb:
             when([ends], lambda: pass_on(0))
-            if q % 2:
+            if detour(q, 3):
                 when([inner], lambda: pass_on(3))
 
     def fold(q, k):
         conds = []
-        if hyb and k == 3 and q % 2:
+        if detour(q, k):
             conds = [inner]
         if hyb and k == 2:
             conds = [ends]
@@ -567,35 +576,35 @@
 
         when(conds, add)
 
-    def reduce(q):
-        for k in range(nz - 1, 0, -1):
-            fold(q, k)
-            dz = by_z([near[zz][k] for zz in range(nz)])
-
-            def move(right, far, k=k, dz=dz):
-                def act():
-                    value = acc[k * chunks + q]
-                    mine = dz * chunks + q
-
-                    @pl.when(z == far)
-                    def _():
-                        sent[mine] = value.astype(jnp.bfloat16)
-
-                    @pl.when(z != far)
-                    def _():
-                        z_copy(q, dz, right).wait_recv()
-                        more = got[(dz + right) * chunks + q].astype(jnp.float32)
-                        sent[mine] = (value + more).astype(jnp.bfloat16)
-
-                    z_copy(q, dz, right).start()
-
-                return act
-
-            when([lambda: flag([near[zz][k] > zz for zz in range(nz)])], move(1, 0))
-            when([lambda: flag([near[zz][k] < zz for zz in range(nz)])], move(0, nz - 1))
+    def move_on(q, k):
+        fold(q, k)
+        dz = by_z([near[zz][k] for zz in range(nz)])
+
+        def move(right, far):
+            def act():
+                value = acc[k * chunks + q]
+                mine = dz * chunks + q
+
+                @pl.when(z == far)
+                def _():
+                    sent[mine] = value.astype(jnp.bfloat16)
+
+                @pl.when(z != far)
+                def _():
+                    z_copy(q, dz, right).wait_recv()
+                    more = got[(dz + right) * chunks + q].astype(jnp.float32)
+                    sent[mine] = (value + more).astype(jnp.bfloat16)
+
+                z_copy(q, dz, right).start()
+
+            return act
+
+        when([lambda: flag([near[zz][k] > zz for zz in range(nz)])], move(1, 0))
+        when([lambda: flag([near[zz][k] < zz for zz in range(nz)])], move(0, nz - 1))
+
+    def settle(q):
         fold(q, 0)
 
-    def settle(q):
         @pl.when(z > 0)
         def _():
             z_copy(q, z, 1).wait_recv()
@@ -608,15 +617,68 @@
 
         out_ref[:, cols(q)] = acc[q].astype(jnp.bfloat16)
 
-    for i in range(chunks + ahead):
-        if i < chunks:
-            arrive(pieces + i)
-            multiply(i)
-        if 0 < i <= chunks:
-            relay(i - 1)
-        if i >= ahead:
-            reduce(i - ahead)
-    for q in range(chunks):
+    for j in range(1, nx):
+        partial_sum(0, 0, j)
+    extras(nx + 1, tiles)
+
+    halves = nz // 2
+    first = chunks // 2
+    late = range(first, chunks)
+
+    def sums(q):
+        if q:
+            w_across(pieces + q)
+        for half in reversed(range(halves)):
+            for j in range(1, nx):
+                if q or half:
+                    partial_sum(q, half, j)
+        for half in reversed(range(halves)):
+            own_sum(q, half)
+
+    def move_all(q):
+        for k in range(nz - 1, 0, -1):
+            move_on(q, k)
+
+    gather = lambda q: w_gathered(pieces + q)
+    gather(2)
+    sums(0)
+    sums(1)
+    relay(0)
+    gather(3)
+    sums(2)
+    relay(1)
+    sums(3)
+    relay(2)
+    gather(4)
+    move_all(0)
+    sums(4)
+    gather(5)
+    relay(3)
+    move_all(1)
+    gather(6)
+    sums(5)
+    sums(6)
+    gather(7)
+    move_all(2)
+    sums(7)
+    for k in range(nz - 2, -1, -1):
+        for q in late:
+            for j in range(1, nx):
+                leave(q, j, k)
+            if k == 0:
+                relay(q)
+    for q in range(3, first):
+        move_all(q)
+    for k in range(nz - 1, 0, -1):
+        for q in late:
+            move_on(q, k)
+        if k == nz - 1:
+            settle(0)
+            settle(1)
+        elif k == nz - 2:
+            for q in range(2, first):
+                settle(q)
+    for q in late:
         settle(q)
 
     for conds, copy in log:
@@ -669,7 +731,6 @@
     side_rows, side_all = side_in.shape
     side_cols = side_all // n_ep
     chunks = 8
-    ahead = 3
     pieces = 2 * local_experts
     piece = width // chunks
     extra = -(-shared_rows // 16) * 16
@@ -688,7 +749,7 @@
 
     bf16, f32 = jnp.bfloat16, jnp.float32
     dma = pltpu.SemaphoreType.DMA
-    dims = (nz, nx, ny, nc, local_experts, pieces, extra, chunks, ahead)
+    dims = (nz, nx, ny, nc, local_experts, pieces, extra, chunks)
     return pl.pallas_call(
         functools.partial(kernel, dims),
         out_shape=jax.ShapeDtypeStruct((tok_count, width), bf16),
@@ -710,9 +771,9 @@
             pltpu.VMEM((n_ep, 8, padded), f32),
             pltpu.VMEM((n_ep, 8, padded), f32),
             pltpu.VMEM((n_ep * tok_count, 8), f32),
-            dma((nz, 1 + nx, 2)),
-            dma((n_ep, 2)),
-            dma((2,)),
+            dma((nz, 1 + nx, 3)),
+            dma((n_ep, 3)),
+            dma((3,)),
             dma((ny, 1 + nc)),
             dma((pieces + chunks, n_tp)),
             dma,

time: 140 us -> 129 us (0.921)
  Pallas kernels: 138 us -> 127 us
    pallas_call x1, Pallas kernels: 138 us -> 127 us  [body(): pl.pallas_call(functools.partial(kernel, dims), out_shape=jax.ShapeDtypeS...]
where the time goes in v2:
time: 129 us
  Pallas kernels  127 us (98%)
  local copies, waits for them, and re-layouts  1.93 us (1%)
    pallas_call x1, Pallas kernels, body(): pl.pallas_call(functools.partial(kernel, dims), out_shape=jax.ShapeDtypeS...  127 us

profile of v2, /device:TPU:0, one launch (start us, length us, event | category | flops | bytes accessed | tf_op | source)
XLA Modules:
  0.0 128.8 jit_solution(8340280571952983477)
XLA Ops:
  0.0 126.9 %layer.1 = bf16[144,2048]{1,0:T(8,128)(2,1)} custom-call(bf16[144,2048]{1,0:T(8,128)(2,1)} %tokens_ref.1, f32[1,2048]{1,0:T(1,128)} %bitcast.10, s32[8,144]{1,0:T(8,128)} %bitcast.11, f32[8,144]{1,0:T(8,128)} %bitcast.12, bf16[16,128]{1,0:T(8,128)(2,1)} %bitcast.13, bf16[256,2048]{1,0:T(8,128)(2,1)} %bitcast.7, bf16[256,2048]{1,0:T(8,128)(2,1)} %bitcast.8, ...), custom_call_target="tpu_custom_call" | custom-call | tf_op jit(solution)/shard_map/layer/pallas_call | solution.py:753
  126.9 1.9 %copy.15 = bf16[144,2048]{1,0:T(8,128)(2,1)} copy(bf16[144,2048]{1,0:T(8,128)(2,1)} %layer.1) | data formatting | bytes 1179648

commit v3 on v2

--- a/solution.py
+++ b/solution.py
@@ -35,7 +35,7 @@
     tokens_ref, gain_ref, ids_ref, route_ref, side_gate_ref,
     gate_ref, up_ref, down_ref, s_gate_ref, s_up_ref, s_down_ref, side_in_ref, side_out_ref,
     out_ref,
-    tok, wall, side, hidden, side_hid, acc, xs, xr, sent, got, hgot, saux, sc, scol,
+    tok, wall, side, hidden, side_hid, acc, xs, xr, sent, got, hgot, saux, sc, scol, out_v,
     tok_send, tok_recv, hyb_send, w_send, w_recv, side_send, side_recv, swap_send, swap_recv,
     local_sem, aux_send, aux_recv, x_send, x_recv, r_send, l_send, z_recv, h_send, h_recv,
 ):
@@ -94,6 +94,8 @@
         pl.semaphore_signal(barrier, inc=1, device_id=((me + j) % n_ep, tp), device_id_type=MESH)
     for j in range(1, n_tp):
         pl.semaphore_signal(barrier, inc=1, device_id=(me, (tp + j) % n_tp), device_id_type=MESH)
+    load = pltpu.make_async_copy(tokens_ref, tok.at[pl.ds(0, tokens_ref.shape[0])], local_sem.at[2])
+    load.start()
 
 
     def slot_rows(s):
@@ -319,7 +321,8 @@
     for p in range(nc):
         pl.when(c == p)(lambda: side_own(p).start())
 
-    values = tokens_ref[...].astype(jnp.float32)
+    load.wait()
+    values = tok[slot_rows(0), :].astype(jnp.float32)
     scale_inv = lax.rsqrt(jnp.mean(values * values, axis=-1, keepdims=True) + norm_eps)
     normed = (values * scale_inv * gain_ref[...]).astype(jnp.bfloat16)
     tok[slot_rows(0), :] = normed
@@ -452,8 +455,7 @@
     w_gathered(pieces)
     for half in range(1, nz // 2):
         cross_wait(half)
-    units(nx + 1, tiles, 0, pieces)
-    w_gathered(pieces + 1)
+    units(nx + 1, tiles, 0, pieces // 2)
     w_across(pieces)
 
 
@@ -615,34 +617,54 @@
             z_copy(q, z, 0).wait_recv()
             acc[q] += got[z * chunks + q].astype(jnp.float32)
 
-        out_ref[:, cols(q)] = acc[q].astype(jnp.bfloat16)
-
-    for j in range(1, nx):
-        partial_sum(0, 0, j)
-    extras(nx + 1, tiles)
+        out_v[:, cols(q)] = acc[q].astype(jnp.bfloat16)
+        pltpu.make_async_copy(out_v.at[:, cols(q)], out_ref.at[:, cols(q)], local_sem.at[2]).start()
 
     halves = nz // 2
     first = chunks // 2
     late = range(first, chunks)
 
-    def sums(q):
-        if q:
-            w_across(pieces + q)
-        for half in reversed(range(halves)):
-            for j in range(1, nx):
-                if q or half:
-                    partial_sum(q, half, j)
+    def own_sums(q):
         for half in reversed(range(halves)):
             own_sum(q, half)
+            if half and detour(q, nz - 1):
+                when([ends], lambda: move_on(q, nz - 1))
+
+    def early(q):
+        for j in range(1, nx):
+            partial_sum(q, 0, j)
+        own_sums(q)
+
+    def rest(q):
+        for half in reversed(range(1, halves)):
+            for j in range(1, nx):
+                partial_sum(q, half, j)
+
+    def sums(q):
+        w_across(pieces + q)
+        rest(q)
+        early(q)
 
     def move_all(q):
-        for k in range(nz - 1, 0, -1):
-            move_on(q, k)
+        if not detour(q, nz - 1):
+            for k in range(nz - 1, 0, -1):
+                move_on(q, k)
+            return
+        when([inner], lambda: move_on(q, 3))
+        for k in (2, 1):
+            when([ends], lambda: move_on(q, k))
+            when([inner], lambda: move_on(q, 3 - k))
 
     gather = lambda q: w_gathered(pieces + q)
+    early(0)
+    gather(1)
+    units(nx + 1, tiles, pieces // 2, pieces)
+    w_across(pieces + 1)
+    early(1)
+    extras(nx + 1, tiles)
     gather(2)
-    sums(0)
-    sums(1)
+    rest(0)
+    rest(1)
     relay(0)
     gather(3)
     sums(2)
@@ -683,6 +705,7 @@
 
     for conds, copy in log:
         when(conds, lambda: copy().wait_send())
+    pltpu.make_async_copy(out_v, out_ref, local_sem.at[2]).wait()
     each_own(lambda way: w_copy(None, y, way), finish)
     for step in range(1, ny):
         each_forward(lambda b, way: w_copy(None, b, way), step, finish, lambda b: None)
@@ -753,9 +776,10 @@
     return pl.pallas_call(
         functools.partial(kernel, dims),
         out_shape=jax.ShapeDtypeStruct((tok_count, width), bf16),
-        in_specs=[pl.BlockSpec(memory_space=pltpu.VMEM)] * 5
+        in_specs=[pl.BlockSpec(memory_space=pl.ANY)]
+        + [pl.BlockSpec(memory_space=pltpu.VMEM)] * 4
         + [pl.BlockSpec(memory_space=pl.ANY)] * 8,
-        out_specs=pl.BlockSpec(memory_space=pltpu.VMEM),
+        out_specs=pl.BlockSpec(memory_space=pl.ANY),
         scratch_shapes=[
             pltpu.VMEM((n_ep * tok_count, width), bf16),
             pltpu.VMEM((n_tp, 3 * (routed + extra), width), bf16),
@@ -771,6 +795,7 @@
             pltpu.VMEM((n_ep, 8, padded), f32),
             pltpu.VMEM((n_ep, 8, padded), f32),
             pltpu.VMEM((n_ep * tok_count, 8), f32),
+            pltpu.VMEM((tok_count, width), bf16),
             dma((nz, 1 + nx, 3)),
             dma((n_ep, 3)),
             dma((3,)),
@@ -780,7 +805,7 @@
             dma,
             dma,
             dma,
-            dma((2,)),
+            dma((3,)),
             dma,
             dma,
             dma,

time: 129 us -> 127 us (0.984)
  Pallas kernels: 127 us -> 124 us
    pallas_call x1, Pallas kernels: 127 us -> 124 us  [body(): pl.pallas_call(functools.partial(kernel, dims), out_shape=jax.ShapeDtypeS...]
where the time goes in v3:
time: 127 us; the launch traced here: 126 us
  Pallas kernels  124 us (98%)
  local copies, waits for them, and re-layouts  1.93 us (2%)
    pallas_call x1, Pallas kernels, body(): pl.pallas_call(functools.partial(kernel, dims), out_shape=jax.ShapeDtypeS...  124 us

profile of v3, /device:TPU:0, one launch (start us, length us, event | category | flops | bytes accessed | tf_op | source)
XLA Modules:
  0.0 126.1 jit_solution(10525930649053538067)
XLA Ops:
  0.0 124.1 %layer.1 = bf16[144,2048]{1,0:T(8,128)(2,1)} custom-call(bf16[144,2048]{1,0:T(8,128)(2,1)} %tokens_ref.1, f32[1,2048]{1,0:T(1,128)} %bitcast.10, s32[8,144]{1,0:T(8,128)} %bitcast.11, f32[8,144]{1,0:T(8,128)} %bitcast.12, bf16[16,128]{1,0:T(8,128)(2,1)} %bitcast.13, bf16[256,2048]{1,0:T(8,128)(2,1)} %bitcast.7, bf16[256,2048]{1,0:T(8,128)(2,1)} %bitcast.8, ...), custom_call_target="tpu_custom_call" | custom-call | tf_op jit(solution)/shard_map/layer/pallas_call | solution.py:776
  124.2 1.9 %copy.15 = bf16[144,2048]{1,0:T(8,128)(2,1)} copy(bf16[144,2048]{1,0:T(8,128)(2,1)} %layer.1) | data formatting | bytes 1179648

commit v4 on v3

--- a/solution.py
+++ b/solution.py
@@ -36,7 +36,7 @@
     gate_ref, up_ref, down_ref, s_gate_ref, s_up_ref, s_down_ref, side_in_ref, side_out_ref,
     out_ref,
     tok, wall, side, hidden, side_hid, acc, xs, xr, sent, got, hgot, saux, sc, scol, out_v,
-    tok_send, tok_recv, hyb_send, w_send, w_recv, side_send, side_recv, swap_send, swap_recv,
+    tok_send, tok_recv, hyb_send, know, w_send, w_recv, side_send, side_recv, swap_send, swap_recv,
     local_sem, aux_send, aux_recv, x_send, x_recv, r_send, l_send, z_recv, h_send, h_recv,
 ):
     nz, nx, ny, nc, local_experts, pieces, extra, chunks = dims
@@ -90,10 +90,23 @@
         return pl.ds(q * piece, piece)
 
     barrier = pltpu.get_barrier_semaphore()
-    for j in range(1, n_ep):
-        pl.semaphore_signal(barrier, inc=1, device_id=((me + j) % n_ep, tp), device_id_type=MESH)
-    for j in range(1, n_tp):
-        pl.semaphore_signal(barrier, inc=1, device_id=(me, (tp + j) % n_tp), device_id_type=MESH)
+
+    def tell(sem, ep, other):
+        pl.semaphore_signal(sem, inc=1, device_id=(ep, other), device_id_type=MESH)
+
+    def tell_near(sem):
+        pl.when(z < nz - 1)(lambda: tell(sem, me + nx, tp))
+        pl.when(z > 0)(lambda: tell(sem, me - nx, tp))
+        for j in range(1, nx):
+            tell(sem, z * nx + (x + j) % nx, tp)
+
+    near_count = by_z([(zz > 0) + (zz < nz - 1) for zz in range(nz)]) + nx - 1
+    tp_count = jnp.where(y > 0, 1, 0) + jnp.where(y < ny - 1, 1, 0) + nc - 1
+    tell_near(barrier)
+    pl.when(y < ny - 1)(lambda: tell(barrier, me, tp + nc))
+    pl.when(y > 0)(lambda: tell(barrier, me, tp - nc))
+    for j in range(1, nc):
+        tell(barrier, me, y * nc + (c + j) % nc)
     load = pltpu.make_async_copy(tokens_ref, tok.at[pl.ds(0, tokens_ref.shape[0])], local_sem.at[2])
     load.start()
 
@@ -327,19 +340,17 @@
     normed = (values * scale_inv * gain_ref[...]).astype(jnp.bfloat16)
     tok[slot_rows(0), :] = normed
 
-    pl.semaphore_wait(barrier, n_ep + n_tp - 2)
-    for p in range(nc):
-        def side_go(p=p):
-            for j in range(1, n_ep):
-                side_copy(j, p).start()
-
-        pl.when(c == p)(side_go)
+    pl.semaphore_wait(barrier, near_count + tp_count)
     for h in range(parts):
         send_block([], 0, h)
+    tell_near(know.at[0])
     for k in range(pieces + chunks):
         for refs in w_parts(k):
             each_own(lambda way: w_copy(k, y, way, refs), start)
 
+    for i in range(1, nz - 1):
+        pl.semaphore_wait(know.at[i - 1], near_count)
+        tell_near(know.at[i])
     side_vector = side_gate_ref[...].astype(jnp.float32)
     lanes = side_vector.shape[1]
     side_vector = jnp.concatenate(
@@ -358,6 +369,13 @@
         gap = sc.shape[2] - rows
         saux[to] = jnp.concatenate([block, jnp.zeros((8, gap), jnp.float32)], axis=1)
     sc[0] = saux[me]
+    pl.semaphore_wait(know.at[nz - 2], near_count)
+    for p in range(nc):
+        def side_go(p=p):
+            for j in range(1, n_ep):
+                side_copy(j, p).start()
+
+        pl.when(c == p)(side_go)
     for k in range(nz):
         for j in range(nx):
             if k or j:
@@ -799,6 +817,7 @@
             dma((nz, 1 + nx, 3)),
             dma((n_ep, 3)),
             dma((3,)),
+            pltpu.SemaphoreType.REGULAR((nz,)),
             dma((ny, 1 + nc)),
             dma((pieces + chunks, n_tp)),
             dma,

time: 127 us -> 126 us (level)
  no operation moved by 1% of the time
where the time goes in v4:
time: 126 us; the launch traced here: 125 us
  Pallas kernels  123 us (98%)
  local copies, waits for them, and re-layouts  1.93 us (2%)
    pallas_call x1, Pallas kernels, body(): pl.pallas_call(functools.partial(kernel, dims), out_shape=jax.ShapeDtypeS...  123 us

profile of v4, /device:TPU:0, one launch (start us, length us, event | category | flops | bytes accessed | tf_op | source)
XLA Modules:
  0.0 125.2 jit_solution(16452154904454008076)
XLA Ops:
  0.0 123.3 %layer.1 = bf16[144,2048]{1,0:T(8,128)(2,1)} custom-call(bf16[144,2048]{1,0:T(8,128)(2,1)} %tokens_ref.1, f32[1,2048]{1,0:T(1,128)} %bitcast.10, s32[8,144]{1,0:T(8,128)} %bitcast.11, f32[8,144]{1,0:T(8,128)} %bitcast.12, bf16[16,128]{1,0:T(8,128)(2,1)} %bitcast.13, bf16[256,2048]{1,0:T(8,128)(2,1)} %bitcast.7, bf16[256,2048]{1,0:T(8,128)(2,1)} %bitcast.8, ...), custom_call_target="tpu_custom_call" | custom-call | tf_op jit(solution)/shard_map/layer/pallas_call | solution.py:794
  123.3 1.9 %copy.15 = bf16[144,2048]{1,0:T(8,128)(2,1)} copy(bf16[144,2048]{1,0:T(8,128)(2,1)} %layer.1) | data formatting | bytes 1179648

commit v5 on v4

--- a/solution.py
+++ b/solution.py
@@ -334,17 +334,19 @@
     for p in range(nc):
         pl.when(c == p)(lambda: side_own(p).start())
 
+    pl.semaphore_wait(barrier, near_count + tp_count)
+    for refs in w_parts(0):
+        each_own(lambda way: w_copy(0, y, way, refs), start)
     load.wait()
     values = tok[slot_rows(0), :].astype(jnp.float32)
     scale_inv = lax.rsqrt(jnp.mean(values * values, axis=-1, keepdims=True) + norm_eps)
     normed = (values * scale_inv * gain_ref[...]).astype(jnp.bfloat16)
     tok[slot_rows(0), :] = normed
 
-    pl.semaphore_wait(barrier, near_count + tp_count)
     for h in range(parts):
         send_block([], 0, h)
     tell_near(know.at[0])
-    for k in range(pieces + chunks):
+    for k in range(1, pieces + chunks):
         for refs in w_parts(k):
             each_own(lambda way: w_copy(k, y, way, refs), start)
 

time: 126 us -> 126 us (level)
  no operation moved by 1% of the time
where the time goes in v5:
time: 126 us; the launch traced here: 125 us
  Pallas kernels  124 us (98%)
  local copies, waits for them, and re-layouts  1.93 us (2%)
    pallas_call x1, Pallas kernels, body(): pl.pallas_call(functools.partial(kernel, dims), out_shape=jax.ShapeDtypeS...  124 us

profile of v5, /device:TPU:0, one launch (start us, length us, event | category | flops | bytes accessed | tf_op | source)
XLA Modules:
  0.0 125.4 jit_solution(6960921727827400911)
XLA Ops:
  0.0 123.5 %layer.1 = bf16[144,2048]{1,0:T(8,128)(2,1)} custom-call(bf16[144,2048]{1,0:T(8,128)(2,1)} %tokens_ref.1, f32[1,2048]{1,0:T(1,128)} %bitcast.10, s32[8,144]{1,0:T(8,128)} %bitcast.11, f32[8,144]{1,0:T(8,128)} %bitcast.12, bf16[16,128]{1,0:T(8,128)(2,1)} %bitcast.13, bf16[256,2048]{1,0:T(8,128)(2,1)} %bitcast.7, bf16[256,2048]{1,0:T(8,128)(2,1)} %bitcast.8, ...), custom_call_target="tpu_custom_call" | custom-call | tf_op jit(solution)/shard_map/layer/pallas_call | solution.py:796
  123.5 1.9 %copy.15 = bf16[144,2048]{1,0:T(8,128)(2,1)} copy(bf16[144,2048]{1,0:T(8,128)(2,1)} %layer.1) | data formatting | bytes 1179648
